TPU v7x, 32 devices: a whole 2x2x4 slice. The times are simulated.
32 devices in a mesh: rep: 2 (over x), fs: 8 (over z, y), tp: 2 (over core).
Axes of the slice: x: 2, y: 2, z: 4, core: 2. Of those that a mesh axis runs over, the one named last changes fastest.
Arguments:
- pre_gate: bfloat16 [12288, 4096], P(('rep', 'fs'), 'tp'), may hold values from -6 to 6
- pre_linear: bfloat16 [12288, 4096], P(('rep', 'fs'), 'tp'), may hold values from -6 to 6
- taps_gate: float32 [3, 4096], P(None, 'tp'), may hold values from -3.5 to 3.5
- taps_linear: float32 [3, 4096], P(None, 'tp'), may hold values from -3.5 to 3.5
- bias_gate: float32 [4096], P('tp'), may hold values from -3 to 3
- bias_linear: float32 [4096], P('tp'), may hold values from -3 to 3
- down_weight: bfloat16 [4096, 2048], P('tp', 'fs'), may hold values from -0.09375 to 0.09375
- out_grad: bfloat16 [12288, 2048], P(('rep', 'fs')), may hold values from -8 to 8
Outputs:
- grad_gate: bfloat16 [12288, 4096], P(('rep', 'fs'), 'tp')
- grad_linear: bfloat16 [12288, 4096], P(('rep', 'fs'), 'tp')
- grad_taps_gate: float32 [3, 4096], P(None, 'tp')
- grad_taps_linear: float32 [3, 4096], P(None, 'tp')
- grad_bias_gate: float32 [4096], P('tp')
- grad_bias_linear: float32 [4096], P('tp')
- grad_down: float32 [4096, 2048], P('tp', 'fs')
- row_norms: float32 [4096], P('tp')
All inputs are finite; a program needn't handle non-finite values.
Results may differ from a plain program's by a relative error of at most 0.0031.
Values may be sent and summed in bfloat16 or wider, within the bound.
No kernel may reach another device: no remote copies, remote signals or barrier semaphores. Data moves between devices by JAX's collectives and lax.ppermute only.
A program may use at most 128 MiB of HBM per device.

v0:
```python
import jax
import jax.numpy as jnp
from jax import lax
from jax.sharding import PartitionSpec as P


def convolve(values, taps, bias):
    length = values.shape[0]
    padded = jnp.pad(values, ((2, 0), (0, 0)))
    return (
        taps[0] * padded[0:length]
        + taps[1] * padded[1 : length + 1]
        + taps[2] * padded[2 : length + 2]
        + bias
    )


def convolve_back(grads, taps):
    length = grads.shape[0]
    padded = jnp.pad(grads, ((0, 2), (0, 0)))
    return (
        taps[0] * padded[2 : length + 2]
        + taps[1] * padded[1 : length + 1]
        + taps[2] * padded[0:length]
    )


def tap_grads(grads, values):
    length = values.shape[0]
    padded = jnp.pad(values, ((2, 0), (0, 0)))
    return jnp.stack([jnp.sum(grads * padded[j : j + length], axis=0) for j in range(3)])


def local(
    pre_gate, pre_linear, taps_gate, taps_linear, bias_gate, bias_linear, down_weight, out_grad
):
    gate_in = pre_gate.astype(jnp.float32)
    linear_in = pre_linear.astype(jnp.float32)
    gate_pre = convolve(gate_in, taps_gate, bias_gate)
    linear_pre = convolve(linear_in, taps_linear, bias_linear)
    sigma = jax.nn.sigmoid(gate_pre)
    silu_val = gate_pre * sigma
    hidden = (silu_val * linear_pre).astype(jnp.bfloat16)
    columns = out_grad
    grad_hidden = lax.dot_general(
        columns,
        lax.all_gather(down_weight, "fs", axis=1, tiled=True),
        (((1,), (1,)), ((), ())),
        preferred_element_type=jnp.float32,
    )
    grad_gate_pre = grad_hidden * linear_pre * sigma * (1.0 + gate_pre * (1.0 - sigma))
    grad_linear_pre = grad_hidden * silu_val
    grad_gate = convolve_back(grad_gate_pre, taps_gate).astype(jnp.bfloat16)
    grad_linear = convolve_back(grad_linear_pre, taps_linear).astype(jnp.bfloat16)
    conv_parts = (
        tap_grads(grad_gate_pre, gate_in),
        tap_grads(grad_linear_pre, linear_in),
        jnp.sum(grad_gate_pre, axis=0),
        jnp.sum(grad_linear_pre, axis=0),
    )
    grad_taps_gate, grad_taps_linear, grad_bias_gate, grad_bias_linear = lax.psum(
        (conv_parts[0], conv_parts[1], conv_parts[2], conv_parts[3]), ("rep", "fs")
    )
    columns = out_grad
    partial_grad = lax.psum_scatter(
        lax.dot_general(
            columns, hidden, (((0,), (0,)), ((), ())), preferred_element_type=jnp.float32
        ),
        "fs",
        scatter_dimension=0,
        tiled=True,
    )
    summed = lax.psum(partial_grad, "rep")
    grad_down = summed.T
    row_norms = lax.psum(jnp.sum(grad_down * grad_down, axis=1), "fs")
    return (
        grad_gate,
        grad_linear,
        grad_taps_gate,
        grad_taps_linear,
        grad_bias_gate,
        grad_bias_linear,
        grad_down,
        row_norms,
    )


def solution(mesh):
    in_specs = (
        P(("rep", "fs"), "tp"),
        P(("rep", "fs"), "tp"),
        P(None, "tp"),
        P(None, "tp"),
        P("tp"),
        P("tp"),
        P("tp", "fs"),
        P(("rep", "fs"), None),
    )
    out_specs = (
        P(("rep", "fs"), "tp"),
        P(("rep", "fs"), "tp"),
        P(None, "tp"),
        P(None, "tp"),
        P("tp"),
        P("tp"),
        P("tp", "fs"),
        P("tp"),
    )
    return jax.shard_map(local, mesh=mesh, in_specs=in_specs, out_specs=out_specs, check_vma=False)
```

profile of v0, /device:TPU:0, one launch (start us, length us, event | category | flops | bytes accessed | tf_op | source)
XLA Modules:
  0.0 668.1 jit_solution(7865275278848254621)
XLA Ops:
  7.2 0.0 copy-start
  7.2 0.0 all-gather.2.cloned.1.call-start
  7.2 0.7 all-gather.2.cloned.1.call-update
  7.9 0.0 reduce-scatter.2.cloned.1.call-start
  8.0 0.0 copy-start.3
  8.0 5.6 convert_element_type.24
  13.5 0.0 copy-done.3
  13.5 0.0 copy-start.4
  13.5 0.0 copy-start.5
  13.5 0.0 copy-start.7
  13.5 3.4 convert_element_type.23
  17.0 0.0 copy-done.4
  17.0 0.0 copy-done.5
  17.0 120.7 %all-gather.2.cloned.1.call-done = bf16[2048,2048]{1,0:T(8,128)(2,1)} async-done(((bf16[2048,256]{1,0:T(8,128)(2,1)}), bf16[2048,2048]{1,0:T(8,128)(2,1)}) %all-gather.2.cloned.1.call-update) | async-done | bytes 8388624 | tf_op jit(solution)/shard_map/all_gather | solution.py:47
  137.7 0.0 copy-done
  137.7 0.0 copy-done.7
  137.7 0.0 copy-start.1
  137.7 0.0 copy-start.2
  137.7 0.0 copy-start.6
  137.8 25.9 %fusion.4 = (f32[2048]{0:T(1024)}, f32[2048]{0:T(1024)S(1)}, f32[2048]{0:T(1024)S(1)}, f32[2048]{0:T(1024)S(1)}, f32[768,2048]{1,0:T(8,128)}, /*index=5*/f32[768,2048]{1,0:T(8,128)}, f32[768,2048]{1,0:T(8,128)}) fusion(bf16[768,2048]{1,0:T(8,128)(2,1)} %param.9, f32[768,2048]{1,0:T(8,128)} %convert_element_type.23, f32[2048]{0:T(1024)S(1)} %copy-done.7, ...), kind=kOutput, calls=%fused_computation.24 | convolution fusion | flops 6472327168 | bytes 46202880 | tf_op jit(solution)/shard_map/dot_general | solution.py:45
  163.7 0.0 copy-done.1
  163.7 0.0 copy-done.2
  163.7 0.0 copy-done.6
  163.7 19.0 %fusion.5 = (f32[2048]{0:T(1024)}, f32[2048]{0:T(1024)S(1)}, f32[2048]{0:T(1024)S(1)}, f32[2048]{0:T(1024)S(1)}, f32[768,2048]{1,0:T(8,128)}, /*index=5*/f32[768,2048]{1,0:T(8,128)}, bf16[768,2048]{1,0:T(8,128)(2,1)}) fusion(bf16[768,2048]{1,0:T(8,128)(2,1)} %param.8, f32[768,2048]{1,0:T(8,128)S(1)} %copy-done.1, f32[768,2048]{1,0:T(8,128)} %get-tuple-element.25, ...), kind=kLoop, calls=%fused_computation.25 | loop fusion | flops 45604864 | bytes 50397184 | tf_op jit(solution)/shard_map/reduce_sum | solution.py:58
  182.7 15.2 %convolution_bitcast_fusion = f32[2048,2048]{0,1:T(8,128)} fusion(bf16[768,2048]{1,0:T(8,128)(2,1)S(1)} %copy-done, f32[768,2048]{1,0:T(8,128)} %get-tuple-element.27, f32[768,2048]{1,0:T(8,128)} %get-tuple-element.25), kind=kOutput, calls=%fused_computation | convolution fusion | flops 6451888128 | bytes 32505856 | tf_op jit(solution)/shard_map/dot_general | solution.py:66
  197.8 0.0 reduce-scatter.2.cloned.1.call-update
  197.9 0.0 all-reduce.8.cloned.1.call-start
  197.9 278.5 %reduce-scatter.2.cloned.1.call-done = f32[256,2048]{0,1:T(8,128)} async-done(((f32[2048,2048]{0,1:T(8,128)}), f32[256,2048]{0,1:T(8,128)}) %reduce-scatter.2.cloned.1.call-update) | async-done | bytes 2097168 | tf_op jit(solution)/shard_map/reduce_scatter | solution.py:65
  476.4 0.0 all-reduce.8.cloned.1.call-update
  476.5 0.0 all-reduce.10.cloned.1.call-start
  476.5 0.7 pad_maximum_fusion
  477.2 9.6 %add_convert_fusion.1 = bf16[768,2048]{1,0:T(8,128)(2,1)} fusion(f32[768,2048]{1,0:T(8,128)} %get-tuple-element.26, f32[2048]{0:T(1024)S(1)} %bitcast.28, f32[2048]{0:T(1024)S(1)} %bitcast.30, f32[2048]{0:T(1024)S(1)} %bitcast.26), kind=kLoop, calls=%fused_computation.9 | loop fusion | flops 9437184 | bytes 9461760 | tf_op jit(solution)/shard_map/convert_element_type | solution.py:53
  486.8 0.0 all-reduce.10.cloned.1.call-update
  486.8 54.0 %all-reduce.8.cloned.1.call-done = f32[2048,256]{1,0:T(8,128)} async-done(((f32[2048,256]{1,0:T(8,128)}), f32[2048,256]{1,0:T(8,128)}) %all-reduce.8.cloned.1.call-update) | async-done | bytes 2097168 | tf_op jit(solution)/shard_map/psum | solution.py:73
  540.8 1.9 multiply_reduce_fusion.6
  542.8 22.3 %psum.47 = f32[2048]{0:T(1024)} all-reduce(f32[2048]{0:T(1024)S(1)} %multiply_reduce_fusion.6), channel_id=1, replica_groups=mesh['rep'=2,'fs'=8,'tp'=2] {'fs'}, use_global_device_ids=true, to_apply=%region_15.16 | all-reduce | flops 2048 | bytes 16384 | tf_op jit(solution)/shard_map/psum | solution.py:75
  565.1 88.1 %all-reduce.10.cloned.1.call-done = (f32[3,2048]{1,0:T(4,128)}, f32[3,2048]{1,0:T(4,128)}, f32[2048]{0:T(1024)}, f32[2048]{0:T(1024)}) async-done(((f32[3,2048]{1,0:T(4,128)}, f32[3,2048]{1,0:T(4,128)}, f32[2048]{0:T(1024)}, f32[2048]{0:T(1024)}), (f32[3,2048]{1,0:T(4,128)}, f32[3,2048]{1,0:T(4,128)}, f32[2048]{0:T(1024)}, f32[2048]{0:T(1024)})) %all-reduce.10.cloned.1.call-update) | async-done | bytes 65552 | tf_op jit(solution)/shard_map/psum | solution.py:61
  653.2 1.4 copy.21
  654.6 1.4 copy.22
  655.9 1.3 copy.23
  657.2 1.3 copy.24
  658.5 3.0 copy.25
  (2 shorter events, 0.0 us)
Async XLA Ops:
  7.2 130.6 %copy-start = (bf16[768,2048]{1,0:T(8,128)(2,1)S(1)}, bf16[768,2048]{1,0:T(8,128)(2,1)}, u32[]{:S(2)}) copy-start(bf16[768,2048]{1,0:T(8,128)(2,1)} %param.15) | copy-start | bytes 9437188
  7.2 130.5 %all-gather.2.cloned.1.call-start = ((), (), s32[]{:S(2)}) async-start(), calls=%async_computation.1 | async-start | bytes 9437184 | tf_op jit(solution)/shard_map/all_gather | solution.py:47
  7.9 468.5 %reduce-scatter.2.cloned.1.call-start = ((), (), s32[]{:S(2)}) async-start(), calls=%async_computation.2 | async-start | bytes 18874368 | tf_op jit(solution)/shard_map/reduce_scatter | solution.py:65
  8.0 5.6 copy-start.3
  13.5 3.4 copy-start.4
  13.5 3.5 copy-start.5
  13.5 124.2 %copy-start.7 = (f32[2048]{0:T(1024)S(1)}, f32[2048]{0:T(1024)}, u32[]{:S(2)}) copy-start(f32[2048]{0:T(1024)} %param.12) | copy-start | bytes 24580
  137.7 25.9 %copy-start.1 = (f32[768,2048]{1,0:T(8,128)S(1)}, f32[768,2048]{1,0:T(8,128)}, u32[]{:S(2)}) copy-start(f32[768,2048]{1,0:T(8,128)} %convert_element_type.24) | copy-start | bytes 18874372
  137.7 25.9 %copy-start.2 = (f32[768,2048]{1,0:T(8,128)S(1)}, f32[768,2048]{1,0:T(8,128)}, u32[]{:S(2)}) copy-start(f32[768,2048]{1,0:T(8,128)} %convert_element_type.23) | copy-start | bytes 18874372
  137.7 25.9 %copy-start.6 = (f32[2048]{0:T(1024)S(1)}, f32[2048]{0:T(1024)}, u32[]{:S(2)}) copy-start(f32[2048]{0:T(1024)} %param.13) | copy-start | bytes 24580
  197.9 343.0 %all-reduce.8.cloned.1.call-start = ((), (), s32[]{:S(2)}) async-start(), calls=%async_computation.3 | async-start | bytes 4194304 | tf_op jit(solution)/shard_map/psum | solution.py:73
  476.5 176.7 %all-reduce.10.cloned.1.call-start = ((), (), s32[]{:S(2)}) async-start(), calls=%async_computation.4 | async-start | bytes 163840 | tf_op jit(solution)/shard_map/psum | solution.py:61
Sparse Core Ops, SparseCore 0:
  10.0 127.6 all-gather.1
  198.0 278.3 reduce-scatter.1
  478.7 62.0 all-reduce.7
  547.2 105.9 all-reduce.9
where the time goes:
time: 669 us; the launch traced here: 668 us
  waiting for transfers between devices  542 us (81%)
  matrix products  41.1 us (6%)
  other arithmetic  40.2 us (6%)
  blocking collectives  22.3 us (3%)
  between operations  13.8 us (2%)
  local copies, waits for them, and re-layouts  8.47 us (1%)
    reduce_scatter x1, waiting for transfers between devices, local(): lax.psum_scatter(lax.dot_general(columns, hidden, (((0,), (0,)), ((), ())...  279 us
    all_gather x1, waiting for transfers between devices, local(): lax.all_gather(down_weight, 'fs', axis=1, tiled=True)  121 us
    psum x1, waiting for transfers between devices, local(): lax.psum((conv_parts[0], conv_parts[1], conv_parts[2], conv_parts[3]), ('...  88.1 us
    psum x1, waiting for transfers between devices, local(): summed = lax.psum(partial_grad, 'rep')  54 us
    dot_general x1, matrix products, local(): lax.dot_general(columns, lax.all_gather(down_weight, 'fs', axis=1, tiled=...  25.9 us
    psum x1, blocking collectives, local(): row_norms = lax.psum(jnp.sum(grad_down * grad_down, axis=1), 'fs')  22.3 us
    reduce_sum x1, other arithmetic, local(): jnp.sum(grad_gate_pre, axis=0)  19 us
    dot_general x1, matrix products, local(): lax.dot_general(columns, hidden, (((0,), (0,)), ((), ())), preferred_elem...  15.2 us
  transfers between devices with their start and end apart: 4, of which 4 were waited for; matrix products, arithmetic and copies ran while one was open for 3% of the time, Pallas kernels for 0%

commit v1 on v0

--- a/solution.py
+++ b/solution.py
@@ -58,8 +58,8 @@
         jnp.sum(grad_gate_pre, axis=0),
         jnp.sum(grad_linear_pre, axis=0),
     )
-    grad_taps_gate, grad_taps_linear, grad_bias_gate, grad_bias_linear = lax.psum(
-        (conv_parts[0], conv_parts[1], conv_parts[2], conv_parts[3]), ("rep", "fs")
+    grad_taps_gate, grad_taps_linear, grad_bias_gate, grad_bias_linear = jax.lax.psum(
+        jax.lax.psum((conv_parts[0], conv_parts[1], conv_parts[2], conv_parts[3]), "fs"), "rep"
     )
     columns = out_grad
     partial_grad = lax.psum_scatter(

time: 669 us -> 656 us (0.981)
  blocking collectives: 22.3 us -> 0 us
  waiting for transfers between devices: 542 us -> 550 us
    psum x1 -> x0, blocking collectives: 22.3 us -> none  [local(): row_norms = lax.psum(jnp.sum(grad_down * grad_down, axis=1), 'fs')]
    psum x1, waiting for transfers between devices: 54 us -> 63.7 us  [local(): summed = lax.psum(partial_grad, 'rep')]
    psum x1 -> x2, waiting for transfers between devices: 88.1 us -> 86.4 us  [the longest x1 73.2 us: local(): jax.lax.psum((conv_parts[0], conv_parts[1], conv_parts[2], conv_parts[3])...]
  transfers between devices with their start and end apart: 4 -> 5, of which waited for: 4 -> 5; matrix products, arithmetic and copies ran while one was open for 3% -> 3% of each run, Pallas kernels for 0% -> 0%
where the time goes in v1:
time: 656 us; the launch traced here: 655 us
  waiting for transfers between devices  550 us (84%)
  matrix products  41.1 us (6%)
  other arithmetic  41 us (6%)
  between operations  13.9 us (2%)
  local copies, waits for them, and re-layouts  9.07 us (1%)
    reduce_scatter x1, waiting for transfers between devices, local(): lax.psum_scatter(lax.dot_general(columns, hidden, (((0,), (0,)), ((), ())...  279 us
    all_gather x1, waiting for transfers between devices, local(): lax.all_gather(down_weight, 'fs', axis=1, tiled=True)  121 us
    psum x1, waiting for transfers between devices, local(): jax.lax.psum((conv_parts[0], conv_parts[1], conv_parts[2], conv_parts[3])...  73.2 us
    psum x1, waiting for transfers between devices, local(): summed = lax.psum(partial_grad, 'rep')  63.7 us
    dot_general x1, matrix products, local(): lax.dot_general(columns, lax.all_gather(down_weight, 'fs', axis=1, tiled=...  25.9 us
    reduce_sum x1, other arithmetic, local(): jnp.sum(grad_gate_pre, axis=0)  19.5 us
    dot_general x1, matrix products, local(): lax.dot_general(columns, hidden, (((0,), (0,)), ((), ())), preferred_elem...  15.2 us
    psum x1, waiting for transfers between devices, local(): jax.lax.psum(jax.lax.psum((conv_parts[0], conv_parts[1], conv_parts[2], c...  13.2 us
  transfers between devices with their start and end apart: 5, of which 5 were waited for; matrix products, arithmetic and copies ran while one was open for 3% of the time, Pallas kernels for 0%

profile of v1, /device:TPU:0, one launch (start us, length us, event | category | flops | bytes accessed | tf_op | source)
XLA Modules:
  0.0 655.3 jit_solution(3258698762246823246)
XLA Ops:
  7.2 0.0 copy-start
  7.2 0.0 all-gather.2.cloned.1.call-start
  7.2 0.7 all-gather.2.cloned.1.call-update
  7.9 0.0 reduce-scatter.2.cloned.1.call-start
  8.0 0.0 copy-start.3
  8.0 5.5 convert_element_type.24
  13.4 0.0 copy-done.3
  13.4 0.0 copy-start.4
  13.4 0.0 copy-start.5
  13.4 0.0 copy-start.8
  13.5 3.4 convert_element_type.23
  16.9 0.0 copy-done.4
  16.9 0.0 copy-done.5
  16.9 120.8 %all-gather.2.cloned.1.call-done = bf16[2048,2048]{1,0:T(8,128)(2,1)} async-done(((bf16[2048,256]{1,0:T(8,128)(2,1)}), bf16[2048,2048]{1,0:T(8,128)(2,1)}) %all-gather.2.cloned.1.call-update) | async-done | bytes 8388624 | tf_op jit(solution)/shard_map/all_gather | solution.py:47
  137.7 0.0 copy-done
  137.7 0.0 copy-done.8
  137.7 0.0 copy-start.1
  137.7 0.0 copy-start.2
  137.7 0.0 copy-start.6
  137.8 25.9 %fusion.4 = (f32[2048]{0:T(1024)}, f32[2048]{0:T(1024)S(1)}, f32[2048]{0:T(1024)S(1)}, f32[2048]{0:T(1024)S(1)}, f32[768,2048]{1,0:T(8,128)}, /*index=5*/f32[768,2048]{1,0:T(8,128)}, f32[768,2048]{1,0:T(8,128)}) fusion(bf16[768,2048]{1,0:T(8,128)(2,1)} %param.9, f32[768,2048]{1,0:T(8,128)} %convert_element_type.23, f32[2048]{0:T(1024)S(1)} %copy-done.8, ...), kind=kOutput, calls=%fused_computation.24 | convolution fusion | flops 6472327168 | bytes 46202880 | tf_op jit(solution)/shard_map/dot_general | solution.py:45
  163.7 0.0 copy-done.1
  163.7 0.0 copy-done.2
  163.7 0.0 copy-done.6
  163.7 19.5 %fusion.5 = (f32[2048]{0:T(1024)}, f32[2048]{0:T(1024)S(1)}, f32[2048]{0:T(1024)S(1)}, f32[2048]{0:T(1024)S(1)}, f32[768,2048]{1,0:T(8,128)}, /*index=5*/f32[768,2048]{1,0:T(8,128)}, bf16[768,2048]{1,0:T(8,128)(2,1)}) fusion(bf16[768,2048]{1,0:T(8,128)(2,1)} %param.8, f32[768,2048]{1,0:T(8,128)S(1)} %copy-done.1, f32[768,2048]{1,0:T(8,128)} %get-tuple-element.30, ...), kind=kLoop, calls=%fused_computation.25 | loop fusion | flops 45604864 | bytes 50397184 | tf_op jit(solution)/shard_map/reduce_sum | solution.py:58
  183.2 15.2 %convolution_bitcast_fusion = f32[2048,2048]{0,1:T(8,128)} fusion(bf16[768,2048]{1,0:T(8,128)(2,1)S(1)} %copy-done, f32[768,2048]{1,0:T(8,128)} %get-tuple-element.32, f32[768,2048]{1,0:T(8,128)} %get-tuple-element.30), kind=kOutput, calls=%fused_computation | convolution fusion | flops 6451888128 | bytes 32505856 | tf_op jit(solution)/shard_map/dot_general | solution.py:66
  198.3 0.0 reduce-scatter.2.cloned.1.call-update
  198.4 0.0 all-reduce.10.cloned.1.call-start
  198.4 278.5 %reduce-scatter.2.cloned.1.call-done = f32[256,2048]{0,1:T(8,128)} async-done(((f32[2048,2048]{0,1:T(8,128)}), f32[256,2048]{0,1:T(8,128)}) %reduce-scatter.2.cloned.1.call-update) | async-done | bytes 2097168 | tf_op jit(solution)/shard_map/reduce_scatter | solution.py:65
  476.9 0.0 all-reduce.10.cloned.1.call-update
  476.9 0.0 all-reduce.12.cloned.1.call-start
  477.0 0.7 pad_maximum_fusion
  477.7 63.7 %all-reduce.10.cloned.1.call-done = f32[2048,256]{1,0:T(8,128)} async-done(((f32[2048,256]{1,0:T(8,128)}), f32[2048,256]{1,0:T(8,128)}) %all-reduce.10.cloned.1.call-update) | async-done | bytes 2097168 | tf_op jit(solution)/shard_map/psum | solution.py:73
  541.3 2.5 multiply_reduce_fusion.6
  543.9 0.0 all-reduce.12.cloned.1.call-update
  543.9 0.0 all-reduce.14.cloned.1.call-start
  543.9 73.2 %all-reduce.12.cloned.1.call-done = (f32[3,2048]{1,0:T(4,128)}, f32[3,2048]{1,0:T(4,128)}, f32[2048]{0:T(1024)}, f32[2048]{0:T(1024)}, f32[2048]{0:T(1024)}) async-done(((f32[3,2048]{1,0:T(4,128)}, f32[3,2048]{1,0:T(4,128)}, f32[2048]{0:T(1024)}, f32[2048]{0:T(1024)}, f32[2048]{0:T(1024)}), (f32[3,2048]{1,0:T(4,128)}, f32[3,2048]{1,0:T(4,128)}, f32[2048]{0:T(1024)}, f32[2048]{0:T(1024)}, ...) | async-done | bytes 73744 | tf_op jit(solution)/shard_map/psum | solution.py:62
  617.1 0.0 all-reduce.14.cloned.1.call-update
  617.1 0.0 copy-start.7
  617.1 9.4 %add_convert_fusion.1 = bf16[768,2048]{1,0:T(8,128)(2,1)} fusion(f32[768,2048]{1,0:T(8,128)} %get-tuple-element.31, f32[2048]{0:T(1024)S(1)} %bitcast.28, f32[2048]{0:T(1024)S(1)} %bitcast.30, f32[2048]{0:T(1024)S(1)} %bitcast.26), kind=kLoop, calls=%fused_computation.9 | loop fusion | flops 9437184 | bytes 9461760 | tf_op jit(solution)/shard_map/convert_element_type | solution.py:53
  626.6 13.2 %all-reduce.14.cloned.1.call-done = (f32[3,2048]{1,0:T(4,128)}, f32[3,2048]{1,0:T(4,128)}, f32[2048]{0:T(1024)}, f32[2048]{0:T(1024)}) async-done(((f32[3,2048]{1,0:T(4,128)}, f32[3,2048]{1,0:T(4,128)}, f32[2048]{0:T(1024)}, f32[2048]{0:T(1024)}), (f32[3,2048]{1,0:T(4,128)}, f32[3,2048]{1,0:T(4,128)}, f32[2048]{0:T(1024)}, f32[2048]{0:T(1024)})) %all-reduce.14.cloned.1.call-update) | async-done | bytes 65552 | tf_op jit(solution)/shard_map/psum | solution.py:61
  639.8 1.4 copy.26
  641.1 1.4 copy.27
  642.5 1.3 copy.28
  643.8 1.3 copy.29
  645.1 3.0 copy.30
  648.2 0.0 copy-done.7
  648.2 0.6 copy.31
  (2 shorter events, 0.0 us)
Async XLA Ops:
  7.2 130.6 %copy-start = (bf16[768,2048]{1,0:T(8,128)(2,1)S(1)}, bf16[768,2048]{1,0:T(8,128)(2,1)}, u32[]{:S(2)}) copy-start(bf16[768,2048]{1,0:T(8,128)(2,1)} %param.15) | copy-start | bytes 9437188
  7.2 130.5 %all-gather.2.cloned.1.call-start = ((), (), s32[]{:S(2)}) async-start(), calls=%async_computation.1 | async-start | bytes 9437184 | tf_op jit(solution)/shard_map/all_gather | solution.py:47
  7.9 469.0 %reduce-scatter.2.cloned.1.call-start = ((), (), s32[]{:S(2)}) async-start(), calls=%async_computation.2 | async-start | bytes 18874368 | tf_op jit(solution)/shard_map/reduce_scatter | solution.py:65
  8.0 5.5 copy-start.3
  13.4 3.4 copy-start.4
  13.4 3.5 copy-start.5
  13.4 124.3 %copy-start.8 = (f32[2048]{0:T(1024)S(1)}, f32[2048]{0:T(1024)}, u32[]{:S(2)}) copy-start(f32[2048]{0:T(1024)} %param.12) | copy-start | bytes 24580
  137.7 25.9 %copy-start.1 = (f32[768,2048]{1,0:T(8,128)S(1)}, f32[768,2048]{1,0:T(8,128)}, u32[]{:S(2)}) copy-start(f32[768,2048]{1,0:T(8,128)} %convert_element_type.24) | copy-start | bytes 18874372
  137.7 25.9 %copy-start.2 = (f32[768,2048]{1,0:T(8,128)S(1)}, f32[768,2048]{1,0:T(8,128)}, u32[]{:S(2)}) copy-start(f32[768,2048]{1,0:T(8,128)} %convert_element_type.23) | copy-start | bytes 18874372
  137.7 25.9 %copy-start.6 = (f32[2048]{0:T(1024)S(1)}, f32[2048]{0:T(1024)}, u32[]{:S(2)}) copy-start(f32[2048]{0:T(1024)} %param.13) | copy-start | bytes 24580
  198.4 343.0 %all-reduce.10.cloned.1.call-start = ((), (), s32[]{:S(2)}) async-start(), calls=%async_computation.3 | async-start | bytes 4194304 | tf_op jit(solution)/shard_map/psum | solution.py:73
  476.9 140.2 %all-reduce.12.cloned.1.call-start = ((), (), s32[]{:S(2)}) async-start(), calls=%async_computation.4 | async-start | bytes 180224 | tf_op jit(solution)/shard_map/psum | solution.py:62
  543.9 95.9 %all-reduce.14.cloned.1.call-start = ((), (), s32[]{:S(2)}) async-start(), calls=%async_computation.5 | async-start | bytes 163840 | tf_op jit(solution)/shard_map/psum | solution.py:61
  617.1 31.0 %copy-start.7 = (f32[2048]{0:T(1024)S(1)}, f32[2048]{0:T(1024)}, u32[]{:S(2)}) copy-start(f32[2048]{0:T(1024)} %get-tuple-element.50) | copy-start | bytes 24580
Sparse Core Ops, SparseCore 0:
  10.0 127.6 all-gather.1
  198.5 278.3 reduce-scatter.1
  479.2 62.0 all-reduce.9
  545.7 71.4 all-reduce.11
  619.4 20.3 all-reduce.13
